TPU v7x, 32 devices: a whole 2x2x4 slice. The times are simulated.
32 devices in a mesh: ep: 8 (over z, core), tp: 4 (over y, x).
Axes of the slice: x: 2, y: 2, z: 4, core: 2. Of those that a mesh axis runs over, the one named last changes fastest.
Arguments:
- tokens: bfloat16 [1024, 4096], P('ep', 'tp'), may hold values from -6 to 6
- out_grad: bfloat16 [1024, 4096], P('ep', 'tp'), may hold values from -1.5 to 1.5
- routes: int32 [1024, 2], P('ep'), may hold values from 0 to 7, all different within a row; in each aligned block of 128 rows (0 to 127, 128 to 255, ...) at most 40 rows name the same one
- route_weights: float32 [1024, 2], P('ep'), may hold values from 0.2 to 1.2
- gate_proj: bfloat16 [8, 1024, 4096], P('ep', 'tp'), may hold values from -0.09375 to 0.09375
- up_proj: bfloat16 [8, 1024, 4096], P('ep', 'tp'), may hold values from -0.09375 to 0.09375
- down_proj: bfloat16 [8, 1024, 4096], P('ep', 'tp'), may hold values from -0.1875 to 0.1875
- shared_hidden: bfloat16 [1024, 1024], P('ep'), may hold values from -6 to 6
Outputs:
- token_grad: bfloat16 [1024, 4096], P('ep', 'tp')
- weight_grad: float32 [1024, 2], P('ep')
- gate_grad: bfloat16 [8, 1024, 4096], P('ep', 'tp')
- up_grad: bfloat16 [8, 1024, 4096], P('ep', 'tp')
- down_grad: bfloat16 [8, 1024, 4096], P('ep', 'tp')
- shared_grad: float32 [1024, 4096], P('ep', 'tp')
Inputs may be any that keep to these rules, and one draw needn't show every extreme that they name: Within each block of 128 consecutive tokens, no expert is named by more than 40 routes, and in some blocks one expert is named by exactly 40. The 2 experts of one token differ.
All inputs are finite; a program needn't handle non-finite values.
Results may differ from a plain program's by a relative error of at most 0.0065.
Values may be sent and summed in bfloat16 or wider, within the bound.
A program may use at most 64 MiB of HBM per device.

v0:
```python
import jax
import jax.numpy as jnp
from jax import lax
from jax.sharding import PartitionSpec as P


def slot_tables(routes, num_experts, capacity):
    tok_rows, per_token = routes.shape
    route_count = tok_rows * per_token
    flat_routes = routes.reshape(-1)
    expert_ids = lax.broadcasted_iota(jnp.int32, (route_count, num_experts), 1)
    onehot = (flat_routes[:, None] == expert_ids).astype(jnp.int32)
    slot_rank = jnp.sum((jnp.cumsum(onehot, axis=0) - 1) * onehot, axis=1)
    slot_of_route = flat_routes * capacity + slot_rank
    slot_ids = lax.broadcasted_iota(jnp.int32, (num_experts * capacity, route_count), 0)
    route_ids = lax.broadcasted_iota(jnp.int32, (num_experts * capacity, route_count), 1)
    matches = slot_ids == slot_of_route[None, :]
    route_of_slot = jnp.sum(jnp.where(matches, route_ids, 0), axis=1)
    filled = jnp.any(matches, axis=1)
    return (slot_of_route, route_of_slot, filled)


def local(tokens, out_grad, routes, route_weights, gate_proj, up_proj, down_proj, shared_hidden):
    ep_count = lax.axis_size("ep")
    tp_count = lax.axis_size("tp")
    local_experts = gate_proj.shape[0]
    num_experts = local_experts * ep_count
    tok_rows, per_token = routes.shape
    capacity = max(2, 5 * tok_rows * per_token // (4 * num_experts))
    slot_of_route, route_of_slot, filled = slot_tables(routes, num_experts, capacity)
    token_of_slot = route_of_slot // per_token
    zero_value = jnp.zeros((), jnp.bfloat16)
    slot_weight = jnp.where(filled, route_weights.reshape(-1)[route_of_slot], 0.0)
    slot_weight = slot_weight.astype(jnp.bfloat16).reshape(ep_count, local_experts, capacity)
    layout = (ep_count, local_experts, capacity, -1)
    sent_tokens = jnp.where(filled[:, None], tokens[token_of_slot], zero_value).reshape(layout)
    sent_grads = jnp.where(filled[:, None], out_grad[token_of_slot], zero_value).reshape(layout)
    part_tokens, part_grads, weights_in = (
        lax.all_to_all(sent_tokens, "ep", split_axis=0, concat_axis=2, tiled=True),
        lax.all_to_all(sent_grads, "ep", split_axis=0, concat_axis=2, tiled=True),
        lax.all_to_all(slot_weight, "ep", split_axis=0, concat_axis=2, tiled=True),
    )
    rows_in, grads_in = (
        lax.all_gather(part_tokens, "tp", axis=3, tiled=True),
        lax.all_gather(part_grads, "tp", axis=3, tiled=True),
    )
    rows_in = rows_in[0]
    grads_in = grads_in[0]
    slot_scale = weights_in[0].astype(jnp.float32)
    pre_gate = jnp.einsum("lrd,lfd->lrf", rows_in, gate_proj, preferred_element_type=jnp.float32)
    pre_up = jnp.einsum("lrd,lfd->lrf", rows_in, up_proj, preferred_element_type=jnp.float32)
    squash = jax.nn.sigmoid(pre_gate)
    activated = pre_gate * squash
    hidden = (activated * pre_up).astype(jnp.bfloat16)
    back_grad = jnp.einsum("lrd,lfd->lrf", grads_in, down_proj, preferred_element_type=jnp.float32)
    partial_products = jnp.sum(hidden.astype(jnp.float32) * back_grad, axis=2)
    hidden_grad = slot_scale[:, :, None] * back_grad
    scaled_hidden = (slot_scale[:, :, None] * hidden.astype(jnp.float32)).astype(jnp.bfloat16)
    gate_delta = (hidden_grad * pre_up * squash * (1.0 + pre_gate * (1.0 - squash))).astype(
        jnp.bfloat16
    )
    up_delta = (hidden_grad * activated).astype(jnp.bfloat16)
    gate_grad = jnp.einsum(
        "lrf,lrd->lfd", gate_delta, rows_in, preferred_element_type=jnp.float32
    ).astype(jnp.bfloat16)
    up_grad = jnp.einsum(
        "lrf,lrd->lfd", up_delta, rows_in, preferred_element_type=jnp.float32
    ).astype(jnp.bfloat16)
    down_grad = jnp.einsum(
        "lrf,lrd->lfd", scaled_hidden, grads_in, preferred_element_type=jnp.float32
    ).astype(jnp.bfloat16)
    partial_rows = jnp.einsum(
        "lrf,lfd->lrd", gate_delta, gate_proj, preferred_element_type=jnp.float32
    )
    partial_rows = partial_rows + jnp.einsum(
        "lrf,lfd->lrd", up_delta, up_proj, preferred_element_type=jnp.float32
    )
    partial_rows = partial_rows.astype(jnp.bfloat16)
    gathered = lax.all_to_all(partial_rows, "tp", split_axis=2, concat_axis=0, tiled=True)
    gathered = gathered.reshape((tp_count,) + partial_rows.shape[:2] + (-1,))
    summed = jnp.sum(gathered, axis=0, dtype=jnp.float32)
    products = lax.psum(partial_products, "tp")
    slot_rows, slot_products = (
        lax.all_to_all(summed[None], "ep", split_axis=2, concat_axis=0, tiled=True),
        lax.all_to_all(products[None], "ep", split_axis=2, concat_axis=0, tiled=True),
    )
    feature_width = slot_rows.shape[-1]
    slot_rows = slot_rows.reshape(num_experts * capacity, feature_width)
    route_rows = slot_rows[slot_of_route].reshape(tok_rows, per_token, feature_width)
    token_grad = jnp.sum(route_rows, axis=1).astype(jnp.bfloat16)
    weight_grad = slot_products.reshape(-1)[slot_of_route].reshape(tok_rows, per_token)
    shared_grad = lax.psum_scatter(
        lax.dot_general(
            shared_hidden, out_grad, (((0,), (0,)), ((), ())), preferred_element_type=jnp.float32
        ),
        "ep",
        scatter_dimension=0,
        tiled=True,
    )
    return (token_grad, weight_grad, gate_grad, up_grad, down_grad, shared_grad)


def solution(mesh):
    return jax.shard_map(
        local,
        mesh=mesh,
        in_specs=(
            P("ep", "tp"),
            P("ep", "tp"),
            P("ep", None),
            P("ep", None),
            P("ep", "tp", None),
            P("ep", "tp", None),
            P("ep", "tp", None),
            P("ep", None),
        ),
        out_specs=(
            P("ep", "tp"),
            P("ep", None),
            P("ep", "tp", None),
            P("ep", "tp", None),
            P("ep", "tp", None),
            P("ep", "tp"),
        ),
        check_vma=False,
    )
```

profile of v0, /device:TPU:0, one launch (start us, length us, event | category | flops | bytes accessed | tf_op | source)
XLA Modules:
  0.0 350.5 jit_solution(12991959504227618092)
XLA Ops:
  8.0 0.0 all-gather.5.cloned.1.call-start
  8.1 1.0 copy.50
  9.0 0.1 eq.26
  9.2 0.1 reshape.322
  9.3 0.6 reduce-window.6
  9.9 0.2 slice_reduce_fusion
  10.2 0.1 fusion.26
  10.3 0.2 select_reduce_fusion
  10.4 0.2 fusion.23
  10.6 2.6 gather_fusion.1
  13.3 2.6 gather_fusion.2
  15.9 0.1 broadcast_in_dim.44
  16.0 1.4 broadcast_select_fusion.1
  17.5 24.5 %all_to_all.60 = bf16[8,1,40,1024]{3,2,1,0:T(8,128)(2,1)} all-to-all(bf16[8,1,40,1024]{3,2,1,0:T(8,128)(2,1)S(1)} %get-tuple-element.43), channel_id=1, replica_groups=mesh['ep'=8,'tp'=4] {'ep'}, dimensions={0} | all-to-all | bytes 1310720 | tf_op jit(solution)/shard_map/all_to_all | solution.py:39
  42.0 0.0 all-gather.5.cloned.1.call-update
  42.0 0.0 all-gather.3.cloned.1.call-start
  42.1 21.2 %all_to_all.61 = bf16[8,1,40,1024]{3,2,1,0:T(8,128)(2,1)} all-to-all(bf16[8,1,40,1024]{3,2,1,0:T(8,128)(2,1)S(1)} %get-tuple-element.42), channel_id=1, replica_groups=mesh['ep'=8,'tp'=4] {'ep'}, dimensions={0} | all-to-all | bytes 1310720 | tf_op jit(solution)/shard_map/all_to_all | solution.py:40
  63.3 0.0 reduce-scatter.2.cloned.1.call-start
  63.4 2.8 fusion.30
  66.2 0.0 reduce-scatter.2.cloned.1.call-update
  66.2 0.7 copy-done.10
  66.8 0.1 copy.52
  67.0 0.1 reshape.324
  67.1 2.4 gather_fusion
  69.5 0.1 convert_element_type.110
  69.6 8.1 %all_to_all.62 = bf16[8,1,40]{2,1,0:T(2,128)(2,1)S(1)} all-to-all(bf16[8,1,40]{2,1,0:T(2,128)(2,1)S(1)} %convert_element_type.110), channel_id=1, replica_groups=mesh['ep'=8,'tp'=4] {'ep'}, dimensions={0} | all-to-all | bytes 1280 | tf_op jit(solution)/shard_map/all_to_all | solution.py:41
  77.7 0.1 reshape.335
  77.8 2.8 all-gather.5.cloned.1.call-done
  80.6 2.8 fusion.7
  83.4 0.4 copy-done.6
  83.9 0.9 fusion.9
  84.8 37.3 %all-gather.3.cloned.1.call-done = bf16[1,1,320,4096]{3,2,1,0:T(8,128)(2,1)} async-done(((bf16[1,1,320,1024]{3,2,1,0:T(8,128)(2,1)}), bf16[1,1,320,4096]{3,2,1,0:T(8,128)(2,1)}) %all-gather.3.cloned.1.call-update) | async-done | bytes 2621456 | tf_op jit(solution)/shard_map/all_gather | solution.py:45
  122.0 3.4 fusion.20
  125.4 0.8 fusion.14
  126.3 0.7 copy-done.7
  127.0 2.4 fusion.1
  129.4 14.3 %copy.56 = bf16[1,320,4096]{1,0,2:T(2,128)(2,1)} copy(bf16[1,320,4096]{2,1,0:T(8,128)(2,1)} %fusion.1) | data formatting | bytes 5242880 | tf_op jit(solution)/shard_map/convert_element_type | solution.py:78
  143.7 0.5 broadcast.230
  144.3 68.8 %reduce.16 = bf16[4096,320]{1,0:T(8,128)(2,1)} reduce(bf16[4096,1,320]{2,1,0:T(2,128)(2,1)} %bitcast.67, bf16[]{:T(256)} %broadcast.230), dimensions={1}, to_apply=%bitcast.53.reduce_sub_computation | reduce | bytes 5242882
  213.0 6.1 %reshape.388 = bf16[4,2,163840]{2,1,0:T(2,128)(2,1)} reshape(bf16[4096,320]{1,0:T(8,128)(2,1)} %reduce.16) | data formatting | bytes 5242880
  219.2 4.6 %all-to-all-start.3 = ((bf16[4,2,163840]{2,1,0:T(2,128)(2,1)}), bf16[4,2,163840]{2,1,0:T(2,128)(2,1)}, u32[]{:S(2)}, u32[]{:S(2)}) async-start(bf16[4,2,163840]{2,1,0:T(2,128)(2,1)} %reshape.388), calls=%async_computation.3 | async-start | bytes 5242880 | tf_op jit(solution)/shard_map/all_to_all | solution.py:79
  223.8 33.7 %psum.7 = f32[1,1,320]{2,1,0:T(1,128)S(1)} all-reduce(f32[1,1,320]{2,1,0:T(1,128)S(1)} %broadcast_in_dim.48), channel_id=1, replica_groups=mesh['ep'=8,'tp'=4] {'tp'}, use_global_device_ids=true, to_apply=%region_8.9 | all-reduce | flops 320 | bytes 2560 | tf_op jit(solution)/shard_map/psum | solution.py:82
  257.5 0.8 copy.59
  258.3 4.6 %all-to-all-start.5 = ((f32[1,1,320]{1,0,2:T(1,128)}), f32[1,1,320]{1,0,2:T(1,128)S(1)}, u32[]{:S(2)}, u32[]{:S(2)}) async-start(f32[1,1,320]{1,0,2:T(1,128)} %copy.59), calls=%async_computation.5 | async-start | bytes 327680 | tf_op jit(solution)/shard_map/all_to_all | solution.py:85
  262.9 7.6 %reshape.389 = bf16[4096,1,320]{2,1,0:T(2,128)(2,1)} reshape(bf16[4,2,163840]{2,1,0:T(2,128)(2,1)} %all-to-all-done.3) | data formatting | bytes 5242880
  270.5 14.0 %copy.57 = bf16[1,320,4096]{2,1,0:T(8,128)(2,1)} copy(bf16[1,320,4096]{1,0,2:T(2,128)(2,1)} %bitcast.68) | data formatting | bytes 5242880 | tf_op jit(solution)/shard_map/all_to_all | solution.py:79
  284.5 7.3 %reshape.336 = f32[320,4,1024]{2,1,0:T(4,128)} reshape(bf16[1,320,4096]{2,1,0:T(8,128)(2,1)} %copy.57) | data formatting | bytes 7864320 | tf_op jit(solution)/shard_map/convert_element_type | solution.py:81
  291.8 5.7 %reduce_sum.54 = f32[320,1024]{1,0:T(8,128)S(1)} reduce(f32[320,4,1024]{2,1,0:T(4,128)} %reshape.336, f32[]{:T(128)} %constant.33.clone.1), dimensions={1}, to_apply=%region_5.6 | reduce | flops 983040 | bytes 6553604 | tf_op jit(solution)/shard_map/reduce_sum | solution.py:81
  297.5 2.0 broadcast_in_dim.47
  299.5 5.1 %all-to-all-start.4 = ((f32[1,1,320,1024]{3,1,0,2:T(1,128)}), f32[1,1,320,1024]{3,1,0,2:T(1,128)S(1)}, u32[]{:S(2)}, u32[]{:S(2)}) async-start(f32[1,1,320,1024]{3,1,0,2:T(1,128)} %broadcast_in_dim.47), calls=%async_computation.4 | async-start | bytes 2621440 | tf_op jit(solution)/shard_map/all_to_all | solution.py:84
  304.6 0.1 copy.58
  304.7 0.1 mul.88
  304.9 4.3 %fusion.2 = bf16[1,256,4096]{2,1,0:T(8,128)(2,1)} fusion(bf16[320,256]{1,0:T(8,128)(2,1)S(1)} %get-tuple-element.40, bf16[1,1,320,4096]{3,2,1,0:T(8,128)(2,1)} %all-gather.5.cloned.1.call-done), kind=kOutput, calls=%fused_computation.11 | convolution fusion | flops 672137216 | bytes 4882432 | tf_op jit(solution)/shard_map/lrf,lrd->lfd/dot_general | solution.py:63
  309.3 4.5 %fusion.3 = bf16[1,256,4096]{2,1,0:T(8,128)(2,1)} fusion(bf16[320,256]{1,0:T(8,128)(2,1)S(1)} %get-tuple-element.41, bf16[1,1,320,4096]{3,2,1,0:T(8,128)(2,1)} %all-gather.5.cloned.1.call-done), kind=kOutput, calls=%fused_computation.12 | convolution fusion | flops 672137216 | bytes 4882432 | tf_op jit(solution)/shard_map/lrf,lrd->lfd/dot_general | solution.py:66
  313.7 2.7 fusion.4
  316.4 1.1 reduce.9
  317.5 1.9 gather_fusion.4
  319.4 0.1 reshape.333
  319.6 0.6 copy.60
  320.2 16.6 %all-to-all-done.4 = f32[1,1,320,1024]{3,1,0,2:T(1,128)S(1)} async-done(((f32[1,1,320,1024]{3,1,0,2:T(1,128)}), f32[1,1,320,1024]{3,1,0,2:T(1,128)S(1)}, u32[]{:S(2)}, u32[]{:S(2)}) %all-to-all-start.4) | async-done | bytes 1310752 | tf_op jit(solution)/shard_map/all_to_all | solution.py:84
  336.8 0.3 copy.63
  337.1 2.0 gather_fusion.3
  339.1 1.8 reshape.331
  341.0 2.1 reduce_sum.56
  (35 shorter events, 0.2 us)
Async XLA Ops:
  8.0 72.6 %copy-start = (bf16[1,256,4096]{2,1,0:T(8,128)(2,1)S(1)}, bf16[1,256,4096]{2,1,0:T(8,128)(2,1)}, u32[]{:S(2)}) copy-start(bf16[1,256,4096]{2,1,0:T(8,128)(2,1)} %param.12) | copy-start | bytes 6291460
  8.0 2.6 copy-start.2
  8.0 72.6 %all-gather.5.cloned.1.call-start = ((), (), s32[]{:S(2)}) async-start(), calls=%async_computation.8 | async-start | bytes 3276800 | tf_op jit(solution)/shard_map/all_gather | solution.py:44
  10.6 2.7 copy-start.3
  17.5 45.9 %copy-start.8 = (bf16[128,1024]{1,0:T(8,128)(2,1)S(1)}, bf16[128,1024]{1,0:T(8,128)(2,1)}, u32[]{:S(2)}) copy-start(bf16[128,1024]{1,0:T(8,128)(2,1)} %param.15) | copy-start | bytes 786436
  42.0 80.0 %all-gather.3.cloned.1.call-start = ((), (), s32[]{:S(2)}) async-start(), calls=%async_computation.7 | async-start | bytes 3276800 | tf_op jit(solution)/shard_map/all_gather | solution.py:45
  63.3 279.7 %reduce-scatter.2.cloned.1.call-start = ((), (), s32[]{:S(2)}) async-start(), calls=%async_computation.9 | async-start | bytes 4718592 | tf_op jit(solution)/shard_map/reduce_scatter | solution.py:92
  66.2 0.7 copy-start.10
  80.6 2.8 copy-start.4
  80.6 3.2 copy-start.6
  125.4 1.6 copy-start.7
  219.2 39.1 %all-to-all-start.3 = ((bf16[4,2,163840]{2,1,0:T(2,128)(2,1)}), bf16[4,2,163840]{2,1,0:T(2,128)(2,1)}, u32[]{:S(2)}, u32[]{:S(2)}) async-start(bf16[4,2,163840]{2,1,0:T(2,128)(2,1)} %reshape.388), calls=%async_computation.3 | async-start | bytes 5242880 | tf_op jit(solution)/shard_map/all_to_all | solution.py:79
  258.3 41.2 %all-to-all-start.5 = ((f32[1,1,320]{1,0,2:T(1,128)}), f32[1,1,320]{1,0,2:T(1,128)S(1)}, u32[]{:S(2)}, u32[]{:S(2)}) async-start(f32[1,1,320]{1,0,2:T(1,128)} %copy.59), calls=%async_computation.5 | async-start | bytes 327680 | tf_op jit(solution)/shard_map/all_to_all | solution.py:85
  297.5 7.1 %copy-start.9 = (s32[128,2]{0,1:T(2,128)S(1)}, s32[128,2]{0,1:T(2,128)}, u32[]{:S(2)}) copy-start(s32[128,2]{0,1:T(2,128)} %param.10) | copy-start | bytes 3076
  299.5 37.3 %all-to-all-start.4 = ((f32[1,1,320,1024]{3,1,0,2:T(1,128)}), f32[1,1,320,1024]{3,1,0,2:T(1,128)S(1)}, u32[]{:S(2)}, u32[]{:S(2)}) async-start(f32[1,1,320,1024]{3,1,0,2:T(1,128)} %broadcast_in_dim.47), calls=%async_computation.4 | async-start | bytes 2621440 | tf_op jit(solution)/shard_map/all_to_all | solution.py:84
  309.3 4.5 %copy-start.5 = (bf16[1,1,320,4096]{3,2,1,0:T(8,128)(2,1)S(1)}, bf16[1,1,320,4096]{3,2,1,0:T(8,128)(2,1)}, u32[]{:S(2)}) copy-start(bf16[1,1,320,4096]{3,2,1,0:T(8,128)(2,1)} %all-gather.3.cloned.1.call-done) | copy-start | bytes 7864324
  337.1 6.0 %copy-start.1 = (bf16[1,256,4096]{2,1,0:T(8,128)(2,1)S(1)}, bf16[1,256,4096]{2,1,0:T(8,128)(2,1)}, u32[]{:S(2)}) copy-start(bf16[1,256,4096]{2,1,0:T(8,128)(2,1)} %param.12) | copy-start | bytes 6291460
Sparse Core Ops, SparseCore 0:
  42.1 38.4 all-gather.4
  82.5 39.4 all-gather.2
Sparse Core Ops, SparseCore 1:
  66.7 48.8 reduce-scatter.1
where the time goes:
time: 352 us; the launch traced here: 350 us
  blocking collectives  87.6 us (25%)
  other arithmetic  80.1 us (23%)
  local copies, waits for them, and re-layouts  71.3 us (20%)
  waiting for transfers between devices  56.7 us (16%)
  matrix products  24.6 us (7%)
  between operations  15.7 us (4%)
  starting transfers between devices  14.4 us (4%)
    unnamed x1, other arithmetic  68.8 us
    all_gather x1, waiting for transfers between devices, local(): lax.all_gather(part_grads, 'tp', axis=3, tiled=True)  37.3 us
    psum x1, blocking collectives, local(): products = lax.psum(partial_products, 'tp')  33.7 us
    all_to_all x1, blocking collectives, local(): lax.all_to_all(sent_tokens, 'ep', split_axis=0, concat_axis=2, tiled=True)  24.5 us
    all_to_all x1, blocking collectives, local(): lax.all_to_all(sent_grads, 'ep', split_axis=0, concat_axis=2, tiled=True)  21.2 us
    unnamed x29, local copies, waits for them, and re-layouts  18.1 us
    all_to_all x1, waiting for transfers between devices, local(): lax.all_to_all(summed[None], 'ep', split_axis=2, concat_axis=0, tiled=True)  16.6 us
    convert_element_type x1, local copies, waits for them, and re-layouts, local(): partial_rows = partial_rows.astype(jnp.bfloat16)  14.3 us
  transfers between devices with their start and end apart: 6, of which 3 were waited for; matrix products, arithmetic and copies ran while one was open for 47% of the time, Pallas kernels for 0%

commit v1 on v0

v1 whole, which is shorter than its diff:
```python
import jax
import jax.numpy as jnp
from jax import lax
from jax.sharding import PartitionSpec as P

LANES = 128


def slot_masks(routes, num_experts, capacity):
    tok_rows, per_token = routes.shape
    expert_ids = lax.broadcasted_iota(jnp.int32, (tok_rows, num_experts), 1)
    chosen = [routes[:, k : k + 1] == expert_ids for k in range(per_token)]
    named = sum(c.astype(jnp.bfloat16) for c in chosen)
    before = (
        lax.broadcasted_iota(jnp.int32, (tok_rows, tok_rows), 1)
        < lax.broadcasted_iota(jnp.int32, (tok_rows, tok_rows), 0)
    ).astype(jnp.bfloat16)
    rank = jnp.dot(before, named, preferred_element_type=jnp.float32)
    slots = lax.broadcasted_iota(jnp.int32, (num_experts * capacity, tok_rows), 0)
    masks = []
    for k in range(per_token):
        own_rank = jnp.sum(jnp.where(chosen[k], rank, 0.0), axis=1).astype(jnp.int32)
        masks.append(slots == (routes[:, k] * capacity + own_rank)[None, :])
    return masks


def split_columns(values, width):
    high = values.astype(jnp.bfloat16)
    low = (values - high.astype(jnp.float32)).astype(jnp.bfloat16)
    pair = jnp.stack([high, low], axis=-1)
    return jnp.pad(pair, [(0, 0)] * values.ndim + [(0, width - 2)])


def local(tokens, out_grad, routes, route_weights, gate_proj, up_proj, down_proj, shared_hidden):
    ep_count = lax.axis_size("ep")
    tp_count = lax.axis_size("tp")
    local_experts = gate_proj.shape[0]
    num_experts = local_experts * ep_count
    tok_rows, per_token = routes.shape
    width = tokens.shape[1]
    capacity = max(2, 5 * tok_rows * per_token // (4 * num_experts))
    slot_count = num_experts * capacity
    masks = slot_masks(routes, num_experts, capacity)
    picks = [m.astype(jnp.bfloat16) for m in masks]
    pick = sum(picks)
    weight_b = route_weights.astype(jnp.bfloat16).astype(jnp.float32)
    slot_weight = sum(
        jnp.sum(jnp.where(masks[k], weight_b[:, k][None, :], 0.0), axis=1)
        for k in range(per_token)
    ).astype(jnp.bfloat16)
    sent = jnp.concatenate(
        [
            jnp.dot(pick, tokens, preferred_element_type=jnp.float32).astype(jnp.bfloat16),
            jnp.dot(pick, out_grad, preferred_element_type=jnp.float32).astype(jnp.bfloat16),
            jnp.pad(slot_weight[:, None], ((0, 0), (0, LANES - 1))),
        ],
        axis=1,
    ).reshape(ep_count, local_experts * capacity, 2 * width + LANES)
    came = lax.all_to_all(sent, "ep", split_axis=0, concat_axis=0, tiled=True)
    came = came.reshape(ep_count, local_experts, capacity, -1).transpose(1, 0, 2, 3)
    came = came.reshape(local_experts, ep_count * capacity, -1)
    slot_scale = came[:, :, 2 * width].astype(jnp.float32)
    rows_in = lax.all_gather(came[:, :, :width], "tp", axis=2, tiled=True)
    grads_in = lax.all_gather(came[:, :, width : 2 * width], "tp", axis=2, tiled=True)
    pre_gate = jnp.einsum("lrd,lfd->lrf", rows_in, gate_proj, preferred_element_type=jnp.float32)
    pre_up = jnp.einsum("lrd,lfd->lrf", rows_in, up_proj, preferred_element_type=jnp.float32)
    squash = jax.nn.sigmoid(pre_gate)
    activated = pre_gate * squash
    hidden = (activated * pre_up).astype(jnp.bfloat16)
    back_grad = jnp.einsum("lrd,lfd->lrf", grads_in, down_proj, preferred_element_type=jnp.float32)
    products = jnp.sum(hidden.astype(jnp.float32) * back_grad, axis=2)
    hidden_grad = slot_scale[:, :, None] * back_grad
    scaled_hidden = (slot_scale[:, :, None] * hidden.astype(jnp.float32)).astype(jnp.bfloat16)
    gate_delta = (hidden_grad * pre_up * squash * (1.0 + pre_gate * (1.0 - squash))).astype(
        jnp.bfloat16
    )
    up_delta = (hidden_grad * activated).astype(jnp.bfloat16)
    sides = split_columns(products, LANES)
    blocks = []
    for t in range(tp_count):
        cut = slice(t * width, (t + 1) * width)
        part = jnp.einsum(
            "lrf,lfd->lrd", gate_delta, gate_proj[:, :, cut], preferred_element_type=jnp.float32
        ) + jnp.einsum(
            "lrf,lfd->lrd", up_delta, up_proj[:, :, cut], preferred_element_type=jnp.float32
        )
        blocks.append(jnp.concatenate([part.astype(jnp.bfloat16), sides], axis=2))
    blocks = jnp.stack(blocks)
    parts = lax.all_to_all(blocks, "tp", split_axis=0, concat_axis=0, tiled=True)
    parts = parts.astype(jnp.float32)
    summed = jnp.sum(parts[..., :width], axis=0).astype(jnp.bfloat16)
    total = jnp.sum(parts[..., width] + parts[..., width + 1], axis=0)
    back = jnp.concatenate([summed, split_columns(total, LANES)], axis=2)
    back = back.reshape(local_experts, ep_count, capacity, -1).transpose(1, 0, 2, 3)
    back = back.reshape(ep_count, local_experts * capacity, -1)
    slot_rows = lax.all_to_all(back, "ep", split_axis=0, concat_axis=0, tiled=True)
    slot_rows = slot_rows.reshape(slot_count, -1)
    gate_grad = jnp.einsum(
        "lrf,lrd->lfd", gate_delta, rows_in, preferred_element_type=jnp.float32
    ).astype(jnp.bfloat16)
    up_grad = jnp.einsum(
        "lrf,lrd->lfd", up_delta, rows_in, preferred_element_type=jnp.float32
    ).astype(jnp.bfloat16)
    down_grad = jnp.einsum(
        "lrf,lrd->lfd", scaled_hidden, grads_in, preferred_element_type=jnp.float32
    ).astype(jnp.bfloat16)
    contract_slots = (((0,), (0,)), ((), ()))
    token_grad = lax.dot_general(
        pick, slot_rows[:, :width], contract_slots, preferred_element_type=jnp.float32
    ).astype(jnp.bfloat16)
    tail = slot_rows[:, width:].astype(jnp.float32)
    slot_product = (tail[:, 0] + tail[:, 1])[:, None]
    weight_grad = jnp.stack(
        [jnp.sum(jnp.where(m, slot_product, 0.0), axis=0) for m in masks], axis=1
    )
    shared_grad = lax.psum_scatter(
        lax.dot_general(
            shared_hidden, out_grad, (((0,), (0,)), ((), ())), preferred_element_type=jnp.float32
        ),
        "ep",
        scatter_dimension=0,
        tiled=True,
    )
    return (token_grad, weight_grad, gate_grad, up_grad, down_grad, shared_grad)


def solution(mesh):
    return jax.shard_map(
        local,
        mesh=mesh,
        in_specs=(
            P("ep", "tp"),
            P("ep", "tp"),
            P("ep", None),
            P("ep", None),
            P("ep", "tp", None),
            P("ep", "tp", None),
            P("ep", "tp", None),
            P("ep", None),
        ),
        out_specs=(
            P("ep", "tp"),
            P("ep", None),
            P("ep", "tp", None),
            P("ep", "tp", None),
            P("ep", "tp", None),
            P("ep", "tp"),
        ),
        check_vma=False,
    )
```

time: 352 us -> 224 us (0.64)
  other arithmetic: 80.1 us -> 8.42 us
  local copies, waits for them, and re-layouts: 71.3 us -> 5.51 us
  waiting for transfers between devices: 56.7 us -> 81.9 us
  blocking collectives: 87.6 us -> 77.4 us
  starting transfers between devices: 14.4 us -> 4.73 us
  matrix products: 24.6 us -> 29.5 us
    unnamed x1 -> x0, other arithmetic: 68.8 us -> none
    psum x1 -> x0, blocking collectives: 33.7 us -> none  [local(): products = lax.psum(partial_products, 'tp')]
    all_gather x2, waiting for transfers between devices: 40.1 us -> 71 us  [the longest x1 37.2 us: local(): lax.all_gather(came[:, :, width:2 * width], 'tp', axis=2, tiled=True)]
    all_to_all x3 -> x2, blocking collectives: 53.9 us -> 77.4 us  [the longest x1 40.1 us: local(): came = lax.all_to_all(sent, 'ep', split_axis=0, concat_axis=0, tiled=True)]
    convert_element_type x4 -> x1, local copies, waits for them, and re-layouts: 21.9 us -> 0.11 us  [local(): slot_weight = sum((jnp.sum(jnp.where(masks[k], weight_b[:, k][None, :], 0...]
    unnamed x29 -> x17, local copies, waits for them, and re-layouts: 18.1 us -> 3.12 us
    all_to_all x1 -> x0, local copies, waits for them, and re-layouts: 14 us -> none  [local(): lax.all_to_all(partial_rows, 'tp', split_axis=2, concat_axis=0, tiled=True)]
    gather x5 -> x0, local copies, waits for them, and re-layouts: 11.6 us -> none  [the longest x1 2.64 us: local(): out_grad[token_of_slot]]
  transfers between devices with their start and end apart: 6 -> 4, of which waited for: 3 -> 3; matrix products, arithmetic and copies ran while one was open for 47% -> 15% of each run, Pallas kernels for 0% -> 0%
where the time goes in v1:
time: 224 us; the launch traced here: 223 us
  waiting for transfers between devices  81.9 us (37%)
  blocking collectives  77.4 us (35%)
  matrix products  29.5 us (13%)
  between operations  15.7 us (7%)
  other arithmetic  8.42 us (4%)
  local copies, waits for them, and re-layouts  5.51 us (2%)
  starting transfers between devices  4.73 us (2%)
    all_to_all x1, blocking collectives, local(): came = lax.all_to_all(sent, 'ep', split_axis=0, concat_axis=0, tiled=True)  40.1 us
    all_to_all x1, blocking collectives, local(): lax.all_to_all(blocks, 'tp', split_axis=0, concat_axis=0, tiled=True)  37.3 us
    all_gather x1, waiting for transfers between devices, local(): lax.all_gather(came[:, :, width:2 * width], 'tp', axis=2, tiled=True)  37.2 us
    all_gather x1, waiting for transfers between devices, local(): rows_in = lax.all_gather(came[:, :, :width], 'tp', axis=2, tiled=True)  33.9 us
    all_to_all x1, waiting for transfers between devices, local(): lax.all_to_all(back, 'ep', split_axis=0, concat_axis=0, tiled=True)  10.1 us
    all_to_all x1, starting transfers between devices, local(): lax.all_to_all(back, 'ep', split_axis=0, concat_axis=0, tiled=True)  4.61 us
    dot_general x1, matrix products, local(): jnp.einsum('lrf,lrd->lfd', gate_delta, rows_in, preferred_element_type=jn...  4.49 us
  transfers between devices with their start and end apart: 4, of which 3 were waited for; matrix products, arithmetic and copies ran while one was open for 15% of the time, Pallas kernels for 0%

profile of v1, /device:TPU:0, one launch (start us, length us, event | category | flops | bytes accessed | tf_op | source)
XLA Modules:
  0.0 223.1 jit_solution(4411542689608827784)
XLA Ops:
  8.0 0.0 copy-start
  8.0 0.0 all-gather.5.cloned.1.call-start
  8.1 0.8 slice_bitcast_fusion.3
  8.9 0.7 convert_convert_fusion
  9.6 0.1 select_reduce_fusion.4
  9.7 0.8 convert_add_fusion
  10.5 0.2 select_reduce_fusion.2
  10.7 0.1 convert_element_type.266
  10.8 1.3 convolution_convert_fusion.3
  12.1 1.3 convolution_convert_fusion.4
  13.4 0.1 fusion.17
  13.5 40.1 %all_to_all.15 = bf16[8,40,2176]{2,1,0:T(8,128)(2,1)S(1)} all-to-all(bf16[8,40,2176]{2,1,0:T(8,128)(2,1)S(1)} %bitcast.108), channel_id=1, replica_groups=mesh['ep'=8,'tp'=4] {'ep'}, dimensions={0} | all-to-all | bytes 2785280 | tf_op jit(solution)/shard_map/all_to_all | solution.py:59
  53.6 1.2 fusion.82
  54.8 0.0 all-gather.5.cloned.1.call-update
  54.8 0.0 all-gather.3.cloned.1.call-start
  54.9 0.7 all-gather.3.cloned.1.call-update
  55.6 0.0 reduce-scatter.2.cloned.1.call-start
  55.6 3.8 %fusion.83 = f32[1024,1024]{1,0:T(8,128)} fusion(bf16[128,1024]{1,0:T(8,128)(2,1)} %param.15, bf16[128,1024]{1,0:T(8,128)(2,1)} %param.9), kind=kOutput, calls=%fused_computation.128 | convolution fusion | flops 268435456 | bytes 4718592 | tf_op jit(solution)/shard_map/dot_general | solution.py:117
  59.4 0.0 reduce-scatter.2.cloned.1.call-update
  59.4 0.1 convert_reduce_fusion
  59.6 33.9 %all-gather.5.cloned.1.call-done = bf16[1,320,4096]{2,1,0:T(8,128)(2,1)} async-done(((bf16[1,320,1024]{2,1,0:T(8,128)(2,1)}), bf16[1,320,4096]{2,1,0:T(8,128)(2,1)}) %all-gather.5.cloned.1.call-update) | async-done | bytes 2621456 | tf_op jit(solution)/shard_map/all_gather | solution.py:63
  93.4 0.0 copy-start.2
  93.4 0.0 copy-start.6
  93.4 3.5 %fusion.6 = f32[320,256]{1,0:T(8,128)S(1)} fusion(bf16[1,320,4096]{2,1,0:T(8,128)(2,1)} %all-gather.5.cloned.1.call-done, bf16[1,256,4096]{2,1,0:T(8,128)(2,1)} %param.12), kind=kOutput, calls=%fused_computation.12 | convolution fusion | flops 671088640 | bytes 5046272 | tf_op jit(solution)/shard_map/lrd,lfd->lrf/dot_general | solution.py:65
  96.9 0.0 copy-done.2
  96.9 0.4 copy-done.6
  97.3 0.9 fusion.8
  98.2 37.2 %all-gather.3.cloned.1.call-done = bf16[1,320,4096]{2,1,0:T(8,128)(2,1)} async-done(((bf16[1,320,1024]{2,1,0:T(8,128)(2,1)}), bf16[1,320,4096]{2,1,0:T(8,128)(2,1)}) %all-gather.3.cloned.1.call-update) | async-done | bytes 2621456 | tf_op jit(solution)/shard_map/all_gather | solution.py:64
  135.4 0.0 copy-done
  135.4 2.8 %fusion.56 = (f32[320]{0:T(512)S(1)}, bf16[320,256]{1,0:T(8,128)(2,1)S(1)}, bf16[320,256]{1,0:T(8,128)(2,1)S(1)}, bf16[320,256]{1,0:T(8,128)(2,1)S(1)}) fusion(f32[320,256]{1,0:T(8,128)S(1)} %fusion.8, f32[320,256]{1,0:T(8,128)S(1)} %fusion.6, f32[320]{0:T(512)S(1)} %convert_reduce_fusion, bf16[1,256,4096]{2,1,0:T(8,128)(2,1)S(1)} %copy-done, ...), kind=kOutput, calls=%fused_computation.74 | convolution fusion | flops 672644800 | bytes 5868032 | tf_op jit(solution)/shard_map/lrd,lfd->lrf/dot_general | solution.py:70
  138.2 0.2 copy.26
  138.4 0.0 copy-start.5
  138.4 1.5 fusion.37
  139.9 0.0 copy-start.7
  139.9 1.5 fusion.22
  141.5 0.0 copy-done.5
  141.5 0.3 fusion.40
  141.8 0.0 copy-done.7
  141.8 0.3 fusion.23
  142.2 0.3 fusion.43
  142.5 0.3 fusion.24
  142.9 0.3 fusion.46
  143.2 0.3 fusion.25
  143.5 0.3 fusion.31
  143.8 0.5 pad_maximum_fusion
  144.3 37.3 %all_to_all.16 = bf16[4,1,320,1152]{3,2,1,0:T(8,128)(2,1)S(1)} all-to-all(bf16[4,1,320,1152]{3,2,1,0:T(8,128)(2,1)S(1)} %pad_maximum_fusion), channel_id=1, replica_groups=mesh['ep'=8,'tp'=4] {'tp'}, dimensions={0} | all-to-all | bytes 5898240 | tf_op jit(solution)/shard_map/all_to_all | solution.py:89
  181.6 0.4 convert_element_type.251
  182.0 0.0 copy-start.1
  182.0 2.5 %copy-done.1 = f32[4,1,320,1152]{3,2,1,0:T(8,128)} copy-done((f32[4,1,320,1152]{3,2,1,0:T(8,128)}, f32[4,1,320,1152]{3,2,1,0:T(8,128)S(1)}, u32[]{:S(2)}) %copy-start.1) | copy-done | bytes 5898264
  184.5 0.3 fusion.35
  184.9 0.2 copy.28
  185.1 3.2 %slice_reduce_fusion = bf16[320,1024]{1,0:T(8,128)(2,1)S(1)} fusion(f32[4,1,320,1152]{3,2,1,0:T(8,128)} %copy-done.1), kind=kLoop, calls=%fused_computation | loop fusion | flops 983040 | bytes 5898240 | tf_op jit(solution)/shard_map/reduce_sum | solution.py:91
  188.3 0.9 pad_maximum_fusion.1
  189.2 4.6 %all-to-all-start.2 = ((bf16[8,40,1152]{2,1,0:T(8,128)(2,1)}), bf16[8,40,1152]{2,1,0:T(8,128)(2,1)S(1)}, u32[]{:S(2)}, u32[]{:S(2)}) async-start(bf16[8,40,1152]{2,1,0:T(8,128)(2,1)} %pad_maximum_fusion.1), calls=%async_computation.2 | async-start | bytes 1474560 | tf_op jit(solution)/shard_map/all_to_all | solution.py:96
  193.8 4.5 %fusion = bf16[1,256,4096]{2,1,0:T(8,128)(2,1)} fusion(bf16[320,256]{1,0:T(8,128)(2,1)S(1)} %get-tuple-element.14, bf16[1,320,4096]{2,1,0:T(8,128)(2,1)} %all-gather.5.cloned.1.call-done), kind=kOutput, calls=%fused_computation.4 | convolution fusion | flops 672137216 | bytes 4882432 | tf_op jit(solution)/shard_map/lrf,lrd->lfd/dot_general | solution.py:98
  198.3 0.0 copy-done.3
  198.3 2.6 %fusion.1 = bf16[1,256,4096]{2,1,0:T(8,128)(2,1)} fusion(bf16[320,256]{1,0:T(8,128)(2,1)S(1)} %get-tuple-element.15, bf16[1,320,4096]{2,1,0:T(8,128)(2,1)S(1)} %copy-done.3), kind=kOutput, calls=%fused_computation.5 | convolution fusion | flops 672137216 | bytes 4882432 | tf_op jit(solution)/shard_map/lrf,lrd->lfd/dot_general | solution.py:101
  200.9 0.0 copy-done.4
  200.9 2.7 %fusion.2 = bf16[1,256,4096]{2,1,0:T(8,128)(2,1)} fusion(bf16[1,320,4096]{2,1,0:T(8,128)(2,1)S(1)} %copy-done.4, bf16[320,256]{1,0:T(8,128)(2,1)S(1)} %get-tuple-element.11, f32[320]{0:T(512)S(1)} %convert_reduce_fusion), kind=kOutput, calls=%fused_computation.6 | convolution fusion | flops 672382976 | bytes 4883712 | tf_op jit(solution)/shard_map/lrf,lrd->lfd/dot_general | solution.py:104
  203.6 10.1 %all-to-all-done.2 = bf16[8,40,1152]{2,1,0:T(8,128)(2,1)S(1)} async-done(((bf16[8,40,1152]{2,1,0:T(8,128)(2,1)}), bf16[8,40,1152]{2,1,0:T(8,128)(2,1)S(1)}, u32[]{:S(2)}, u32[]{:S(2)}) %all-to-all-start.2) | async-done | bytes 737312 | tf_op jit(solution)/shard_map/all_to_all | solution.py:96
  213.7 0.2 fusion.60
  213.9 0.1 select_reduce_fusion.1
  214.1 0.6 pad_maximum_fusion.4
  214.6 1.0 convolution_convert_fusion.5
  (13 shorter events, 0.1 us)
Async XLA Ops:
  8.0 127.4 %copy-start = (bf16[1,256,4096]{2,1,0:T(8,128)(2,1)S(1)}, bf16[1,256,4096]{2,1,0:T(8,128)(2,1)}, u32[]{:S(2)}) copy-start(bf16[1,256,4096]{2,1,0:T(8,128)(2,1)} %param.14) | copy-start | bytes 6291460
  8.0 85.4 %all-gather.5.cloned.1.call-start = ((), (), s32[]{:S(2)}) async-start(), calls=%async_computation.5 | async-start | bytes 3276800 | tf_op jit(solution)/shard_map/all_gather | solution.py:63
  54.8 80.6 %all-gather.3.cloned.1.call-start = ((), (), s32[]{:S(2)}) async-start(), calls=%async_computation.4 | async-start | bytes 3276800 | tf_op jit(solution)/shard_map/all_gather | solution.py:64
  55.6 160.1 %reduce-scatter.2.cloned.1.call-start = ((), (), s32[]{:S(2)}) async-start(), calls=%async_computation.6 | async-start | bytes 4718592 | tf_op jit(solution)/shard_map/reduce_scatter | solution.py:116
  93.4 3.5 %copy-start.2 = (bf16[1,320,4096]{2,1,0:T(8,128)(2,1)S(1)}, bf16[1,320,4096]{2,1,0:T(8,128)(2,1)}, u32[]{:S(2)}) copy-start(bf16[1,320,4096]{2,1,0:T(8,128)(2,1)} %all-gather.5.cloned.1.call-done) | copy-start | bytes 7864324
  93.4 3.9 %copy-start.6 = (bf16[1,256,4096]{2,1,0:T(8,128)(2,1)S(1)}, bf16[1,256,4096]{2,1,0:T(8,128)(2,1)}, u32[]{:S(2)}) copy-start(bf16[1,256,4096]{2,1,0:T(8,128)(2,1)} %param.13) | copy-start | bytes 6291460
  138.4 3.1 %copy-start.5 = (bf16[1,256,4096]{2,1,0:T(8,128)(2,1)S(1)}, bf16[1,256,4096]{2,1,0:T(8,128)(2,1)}, u32[]{:S(2)}) copy-start(bf16[1,256,4096]{2,1,0:T(8,128)(2,1)} %param.12) | copy-start | bytes 6291460
  139.9 1.9 copy-start.7
  182.0 2.5 %copy-start.1 = (f32[4,1,320,1152]{3,2,1,0:T(8,128)}, f32[4,1,320,1152]{3,2,1,0:T(8,128)S(1)}, u32[]{:S(2)}) copy-start(f32[4,1,320,1152]{3,2,1,0:T(8,128)S(1)} %convert_element_type.251) | copy-start | bytes 17694724
  189.2 24.5 %all-to-all-start.2 = ((bf16[8,40,1152]{2,1,0:T(8,128)(2,1)}), bf16[8,40,1152]{2,1,0:T(8,128)(2,1)S(1)}, u32[]{:S(2)}, u32[]{:S(2)}) async-start(bf16[8,40,1152]{2,1,0:T(8,128)(2,1)} %pad_maximum_fusion.1), calls=%async_computation.2 | async-start | bytes 1474560 | tf_op jit(solution)/shard_map/all_to_all | solution.py:96
  193.8 4.5 %copy-start.3 = (bf16[1,320,4096]{2,1,0:T(8,128)(2,1)S(1)}, bf16[1,320,4096]{2,1,0:T(8,128)(2,1)}, u32[]{:S(2)}) copy-start(bf16[1,320,4096]{2,1,0:T(8,128)(2,1)} %all-gather.5.cloned.1.call-done) | copy-start | bytes 7864324
  198.3 2.6 %copy-start.4 = (bf16[1,320,4096]{2,1,0:T(8,128)(2,1)S(1)}, bf16[1,320,4096]{2,1,0:T(8,128)(2,1)}, u32[]{:S(2)}) copy-start(bf16[1,320,4096]{2,1,0:T(8,128)(2,1)} %all-gather.3.cloned.1.call-done) | copy-start | bytes 7864324
Sparse Core Ops, SparseCore 0:
  55.0 38.4 all-gather.4
  95.9 39.4 all-gather.2
Sparse Core Ops, SparseCore 1:
  59.5 48.7 reduce-scatter.1

commit v2 on v1

--- a/solution.py
+++ b/solution.py
@@ -1,9 +1,262 @@
+import functools
+
 import jax
 import jax.numpy as jnp
 from jax import lax
+from jax.experimental import pallas as pl
+from jax.experimental.pallas import tpu as pltpu
 from jax.sharding import PartitionSpec as P
 
 LANES = 128
+MESH = pl.DeviceIdType.MESH
+
+
+def greet(me, ep_count, mine, tp_count):
+    barrier = pltpu.get_barrier_semaphore()
+    for d in range(1, ep_count):
+        pl.semaphore_signal(barrier, inc=1, device_id=(me ^ d, mine), device_id_type=MESH)
+    for d in range(1, tp_count):
+        pl.semaphore_signal(barrier, inc=1, device_id=(me, mine ^ d), device_id_type=MESH)
+    pl.semaphore_wait(barrier, ep_count + tp_count - 2)
+
+
+def remote(src, dst, send_sem, recv_sem, target):
+    return pltpu.make_async_remote_copy(
+        src_ref=src,
+        dst_ref=dst,
+        send_sem=send_sem,
+        recv_sem=recv_sem,
+        device_id=target,
+        device_id_type=MESH,
+    )
+
+
+def dispatch_kernel(
+    ep_count, tp_count, width,
+    sent, grads, cols, full, all_grads, all_cols,
+    ep_send, ep_recv, tp_send, tp_recv, col_send, col_recv,
+    up_send, down_send, side_send, shard_recv,
+):
+    me, mine = lax.axis_index("ep"), lax.axis_index("tp")
+    chips, z, core = ep_count // 2, me // 2, me % 2
+    partner = me + 1 - 2 * core
+    relay = tp_count == 4
+    total = sent.shape[-1]
+    halves = [(0, width), (width, total - width)] if relay else [(0, total)]
+    greet(me, ep_count, mine, tp_count)
+    order = sorted(range(1, ep_count), key=lambda d: (d.bit_count(), d))
+
+    def ep_copy(d):
+        return remote(
+            sent.at[me ^ d], full.at[mine, me], ep_send.at[d], ep_recv.at[d], (me ^ d, mine)
+        )
+
+    def col_copy(d):
+        return remote(
+            cols.at[me ^ d], all_cols.at[me], col_send.at[d], col_recv.at[d], (me ^ d, mine)
+        )
+
+    def tp_copy(owner, d, via, h):
+        start, size = halves[h]
+        j = me ^ d
+        cut = pl.ds(start, size)
+        if owner == 0 and d == 0:
+            src = sent.at[me, :, cut]
+        else:
+            src = full.at[mine ^ owner, j, :, cut]
+        lane = owner ^ via
+        return remote(
+            src,
+            full.at[mine ^ owner, j, :, cut],
+            tp_send.at[lane, d, h],
+            tp_recv.at[lane, d, h],
+            (me, mine ^ via),
+        )
+
+    def shard_copy(shard, step, target, sem):
+        src = grads if step == 0 else all_grads.at[shard]
+        return remote(src, all_grads.at[shard], sem, shard_recv.at[shard], (target, mine))
+
+    def guarded(flag, action):
+        pl.when(flag)(action)
+
+    def shard_step(step, waiting=False):
+        act = (lambda c: c.wait_send()) if waiting else (lambda c: c.start())
+        low, high = me - 2 * step, me + 2 * step
+
+        def go_up():
+            act(shard_copy(low, step, me + 2, up_send.at[step]))
+
+        def go_down():
+            act(shard_copy(high, step, me - 2, down_send.at[step]))
+
+        def from_low():
+            if step and not waiting:
+                shard_copy(low, step, partner, side_send.at[0, step]).wait_recv()
+            guarded(z + 1 < chips, go_up)
+            act(shard_copy(low, step, partner, side_send.at[0, step]))
+
+        def from_high():
+            if not waiting:
+                shard_copy(high, step, partner, side_send.at[1, step]).wait_recv()
+            guarded(z > 0, go_down)
+            act(shard_copy(high, step, partner, side_send.at[1, step]))
+
+        if step == 0:
+            from_low()
+            guarded(z > 0, go_down)
+        else:
+            guarded(z - step >= 0, from_low)
+            guarded(z + step < chips, from_high)
+
+    for d in order:
+        ep_copy(d).start()
+    shard_step(0)
+    for d in order:
+        col_copy(d).start()
+    full[mine, me] = sent[me]
+    all_grads[me] = grads[...]
+    all_cols[me] = cols[me]
+
+    def pass_on(d):
+        if relay:
+            tp_copy(1, d, 0, 0).wait_recv()
+            tp_copy(1, d, 2, 0).start()
+            tp_copy(2, d, 0, 1).wait_recv()
+            tp_copy(2, d, 1, 1).start()
+
+    steps = [0] + order
+    shard_at = {ep_count - chips + s: s for s in range(1, chips)}
+    for k, d in enumerate(steps):
+        if d:
+            ep_copy(d).wait_recv()
+        for via in (1, 2) if relay else range(1, tp_count):
+            for h in range(len(halves)):
+                tp_copy(0, d, via, h).start()
+        if k:
+            pass_on(steps[k - 1])
+        if k in shard_at:
+            shard_step(shard_at[k])
+    pass_on(steps[-1])
+    for s in range(1, chips):
+        if s not in shard_at.values():
+            shard_step(s)
+    for d in steps:
+        for via in range(1, tp_count):
+            for h in range(len(halves)):
+                done = not relay or via == 3 or (via, h) not in ((1, 0), (2, 1))
+                if done:
+                    tp_copy(via, d, 0, h).wait_recv()
+    for zz in range(chips):
+        shard_copy(2 * zz + 1 - core, 1, partner, side_send.at[0, 0]).wait_recv()
+    for d in order:
+        col_copy(d).wait_recv()
+        col_copy(d).wait_send()
+        ep_copy(d).wait_send()
+    for s in range(chips):
+        shard_step(s, waiting=True)
+    for d in steps:
+        for via in (1, 2) if relay else range(1, tp_count):
+            for h in range(len(halves)):
+                tp_copy(0, d, via, h).wait_send()
+        if relay:
+            tp_copy(1, d, 2, 0).wait_send()
+            tp_copy(2, d, 1, 1).wait_send()
+
+
+def dispatch(sent, grads, cols, ep_count, tp_count, width):
+    halves = 2 if tp_count == 4 else 1
+    dma = pltpu.SemaphoreType.DMA
+    vmem = pl.BlockSpec(memory_space=pltpu.VMEM)
+    return pl.pallas_call(
+        functools.partial(dispatch_kernel, ep_count, tp_count, width),
+        out_shape=[
+            jax.ShapeDtypeStruct((tp_count,) + sent.shape, sent.dtype),
+            jax.ShapeDtypeStruct((ep_count,) + grads.shape, grads.dtype),
+            jax.ShapeDtypeStruct(cols.shape, cols.dtype),
+        ],
+        in_specs=[vmem] * 3,
+        out_specs=[vmem] * 3,
+        scratch_shapes=[
+            dma((ep_count,)), dma((ep_count,)),
+            dma((tp_count, ep_count, halves)), dma((tp_count, ep_count, halves)),
+            dma((ep_count,)), dma((ep_count,)),
+            dma((ep_count,)), dma((ep_count,)), dma((2, ep_count)), dma((ep_count,)),
+        ],
+        compiler_params=pltpu.CompilerParams(
+            collective_id=0, has_side_effects=True, vmem_limit_bytes=40 * 1024 * 1024
+        ),
+        name="dispatch",
+    )(sent, grads, cols)
+
+
+def combine_kernel(
+    ep_count, tp_count, width, blocks, out, parts, reduced, tp_send, tp_recv, ep_send, ep_recv
+):
+    me, mine = lax.axis_index("ep"), lax.axis_index("tp")
+    greet(me, ep_count, mine, tp_count)
+    order = list(range(ep_count - 1, -1, -1))
+
+    def tp_copy(d, via):
+        return remote(
+            blocks.at[mine ^ via, me ^ d],
+            parts.at[via, d],
+            tp_send.at[via, d],
+            tp_recv.at[via, d],
+            (me, mine ^ via),
+        )
+
+    def ep_copy(d):
+        return remote(reduced.at[d], out.at[me], ep_send.at[d], ep_recv.at[d], (me ^ d, mine))
+
+    for d in order:
+        for via in range(1, tp_count):
+            tp_copy(d, via).start()
+    for d in order:
+        for via in range(1, tp_count):
+            tp_copy(d, via).wait_recv()
+        whole = blocks[mine, me ^ d].astype(jnp.float32)
+        for via in range(1, tp_count):
+            whole = whole + parts[via, d].astype(jnp.float32)
+        high = whole.astype(jnp.bfloat16)
+        side = whole[:, width:]
+        low = (side - high[:, width:].astype(jnp.float32)).astype(jnp.bfloat16)
+        if d:
+            reduced[d, :, : width + LANES] = high
+            reduced[d, :, width + LANES :] = low
+            ep_copy(d).start()
+        else:
+            out[me, :, : width + LANES] = high
+            out[me, :, width + LANES :] = low
+    for d in order:
+        for via in range(1, tp_count):
+            tp_copy(d, via).wait_send()
+        if d:
+            ep_copy(d).wait_recv()
+            ep_copy(d).wait_send()
+
+
+def combine(blocks, ep_count, tp_count, width):
+    rows = blocks.shape[2]
+    dma = pltpu.SemaphoreType.DMA
+    vmem = pl.BlockSpec(memory_space=pltpu.VMEM)
+    final = (ep_count, rows, width + 2 * LANES)
+    return pl.pallas_call(
+        functools.partial(combine_kernel, ep_count, tp_count, width),
+        out_shape=jax.ShapeDtypeStruct(final, blocks.dtype),
+        in_specs=[vmem],
+        out_specs=vmem,
+        scratch_shapes=[
+            pltpu.VMEM(blocks.shape, blocks.dtype),
+            pltpu.VMEM(final, blocks.dtype),
+            dma((tp_count, ep_count)), dma((tp_count, ep_count)),
+            dma((ep_count,)), dma((ep_count,)),
+        ],
+        compiler_params=pltpu.CompilerParams(
+            collective_id=1, has_side_effects=True, vmem_limit_bytes=40 * 1024 * 1024
+        ),
+        name="combine",
+    )(blocks)
 
 
 def slot_masks(routes, num_experts, capacity):
@@ -25,8 +278,9 @@
 
 
 def split_columns(values, width):
-    high = values.astype(jnp.bfloat16)
-    low = (values - high.astype(jnp.float32)).astype(jnp.bfloat16)
+    rounded = lax.reduce_precision(values, 8, 7)
+    high = rounded.astype(jnp.bfloat16)
+    low = (values - rounded).astype(jnp.bfloat16)
     pair = jnp.stack([high, low], axis=-1)
     return jnp.pad(pair, [(0, 0)] * values.ndim + [(0, width - 2)])
 
@@ -56,12 +310,18 @@
         ],
         axis=1,
     ).reshape(ep_count, local_experts * capacity, 2 * width + LANES)
-    came = lax.all_to_all(sent, "ep", split_axis=0, concat_axis=0, tiled=True)
-    came = came.reshape(ep_count, local_experts, capacity, -1).transpose(1, 0, 2, 3)
-    came = came.reshape(local_experts, ep_count * capacity, -1)
-    slot_scale = came[:, :, 2 * width].astype(jnp.float32)
-    rows_in = lax.all_gather(came[:, :, :width], "tp", axis=2, tiled=True)
-    grads_in = lax.all_gather(came[:, :, width : 2 * width], "tp", axis=2, tiled=True)
+    cols = shared_hidden.reshape(tok_rows, ep_count, -1).transpose(1, 0, 2)
+    full, all_grads, all_cols = dispatch(sent, out_grad, cols, ep_count, tp_count, width)
+
+    def features(part):
+        part = part.reshape(tp_count, ep_count, local_experts, capacity, width)
+        part = part.transpose(2, 1, 3, 0, 4)
+        return part.reshape(local_experts, ep_count * capacity, tp_count * width)
+
+    rows_in = features(full[..., :width])
+    grads_in = features(full[..., width : 2 * width])
+    scales = full[0, :, :, 2 * width].reshape(ep_count, local_experts, capacity)
+    slot_scale = scales.transpose(1, 0, 2).reshape(local_experts, -1).astype(jnp.float32)
     pre_gate = jnp.einsum("lrd,lfd->lrf", rows_in, gate_proj, preferred_element_type=jnp.float32)
     pre_up = jnp.einsum("lrd,lfd->lrf", rows_in, up_proj, preferred_element_type=jnp.float32)
     squash = jax.nn.sigmoid(pre_gate)
@@ -85,16 +345,10 @@
             "lrf,lfd->lrd", up_delta, up_proj[:, :, cut], preferred_element_type=jnp.float32
         )
         blocks.append(jnp.concatenate([part.astype(jnp.bfloat16), sides], axis=2))
-    blocks = jnp.stack(blocks)
-    parts = lax.all_to_all(blocks, "tp", split_axis=0, concat_axis=0, tiled=True)
-    parts = parts.astype(jnp.float32)
-    summed = jnp.sum(parts[..., :width], axis=0).astype(jnp.bfloat16)
-    total = jnp.sum(parts[..., width] + parts[..., width + 1], axis=0)
-    back = jnp.concatenate([summed, split_columns(total, LANES)], axis=2)
-    back = back.reshape(local_experts, ep_count, capacity, -1).transpose(1, 0, 2, 3)
-    back = back.reshape(ep_count, local_experts * capacity, -1)
-    slot_rows = lax.all_to_all(back, "ep", split_axis=0, concat_axis=0, tiled=True)
-    slot_rows = slot_rows.reshape(slot_count, -1)
+    blocks = jnp.stack(blocks).reshape(tp_count, local_experts, ep_count, capacity, -1)
+    blocks = blocks.transpose(0, 2, 1, 3, 4)
+    blocks = blocks.reshape(tp_count, ep_count, local_experts * capacity, -1)
+    slot_rows = combine(blocks, ep_count, tp_count, width).reshape(slot_count, -1)
     gate_grad = jnp.einsum(
         "lrf,lrd->lfd", gate_delta, rows_in, preferred_element_type=jnp.float32
     ).astype(jnp.bfloat16)
@@ -109,17 +363,13 @@
         pick, slot_rows[:, :width], contract_slots, preferred_element_type=jnp.float32
     ).astype(jnp.bfloat16)
     tail = slot_rows[:, width:].astype(jnp.float32)
-    slot_product = (tail[:, 0] + tail[:, 1])[:, None]
+    slot_product = tail[:, 0] + tail[:, 1] + tail[:, LANES] + tail[:, LANES + 1]
+    slot_product = slot_product[:, None]
     weight_grad = jnp.stack(
         [jnp.sum(jnp.where(m, slot_product, 0.0), axis=0) for m in masks], axis=1
     )
-    shared_grad = lax.psum_scatter(
-        lax.dot_general(
-            shared_hidden, out_grad, (((0,), (0,)), ((), ())), preferred_element_type=jnp.float32
-        ),
-        "ep",
-        scatter_dimension=0,
-        tiled=True,
+    shared_grad = jnp.einsum(
+        "jth,jtd->hd", all_cols, all_grads, preferred_element_type=jnp.float32
     )
     return (token_grad, weight_grad, gate_grad, up_grad, down_grad, shared_grad)
 

time: 224 us -> 145 us (0.65)
  Pallas kernels: 0 us -> 103 us
  waiting for transfers between devices: 81.9 us -> 0 us
  blocking collectives: 77.4 us -> 0 us
  between operations: 15.7 us -> 0.91 us
  local copies, waits for them, and re-layouts: 5.51 us -> 16.7 us
  matrix products: 29.5 us -> 20.9 us
  other arithmetic: 8.42 us -> 3.1 us
  starting transfers between devices: 4.73 us -> 0 us
    pallas_call x0 -> x2, Pallas kernels: none -> 103 us  [the longest x1 65.8 us: dispatch(): pl.pallas_call(functools.partial(dispatch_kernel, ep_count, tp_count, wid...]
    all_to_all x2 -> x0, blocking collectives: 77.4 us -> none  [the longest x1 40.1 us: local(): came = lax.all_to_all(sent, 'ep', split_axis=0, concat_axis=0, tiled=True)]
    all_gather x2 -> x0, waiting for transfers between devices: 71 us -> none  [the longest x1 37.2 us: local(): lax.all_gather(came[:, :, width:2 * width], 'tp', axis=2, tiled=True)]
    all_to_all x1 -> x0, waiting for transfers between devices: 10.1 us -> none  [local(): lax.all_to_all(back, 'ep', split_axis=0, concat_axis=0, tiled=True)]
    transpose x0 -> x3, local copies, waits for them, and re-layouts: none -> 8.85 us  [features(): part = part.transpose(2, 1, 3, 0, 4)]
    all_to_all x1 -> x0, starting transfers between devices: 4.61 us -> none  [local(): lax.all_to_all(back, 'ep', split_axis=0, concat_axis=0, tiled=True)]
    unnamed x17 -> x25, local copies, waits for them, and re-layouts: 3.12 us -> 6.72 us
    reduce_sum x2 -> x0, other arithmetic: 3.49 us -> none  [the longest x1 3.15 us: local(): summed = jnp.sum(parts[..., :width], axis=0).astype(jnp.bfloat16)]
  transfers between devices with their start and end apart: 4 -> 0, of which waited for: 3 -> 0; matrix products, arithmetic and copies ran while one was open for 15% -> 0% of each run, Pallas kernels for 0% -> 0%
where the time goes in v2:
time: 145 us
  Pallas kernels  103 us (71%)
  matrix products  20.9 us (14%)
  local copies, waits for them, and re-layouts  16.7 us (12%)
  other arithmetic  3.1 us (2%)
    pallas_call x1, Pallas kernels, dispatch(): pl.pallas_call(functools.partial(dispatch_kernel, ep_count, tp_count, wid...  65.8 us
    pallas_call x1, Pallas kernels, combine(): pl.pallas_call(functools.partial(combine_kernel, ep_count, tp_count, widt...  37.5 us
    transpose x3, local copies, waits for them, and re-layouts, features(): part = part.transpose(2, 1, 3, 0, 4)  8.85 us
    unnamed x25, local copies, waits for them, and re-layouts  6.72 us
    dot_general x1, matrix products, local(): jnp.einsum('lrf,lrd->lfd', up_delta, rows_in, preferred_element_type=jnp....  4.49 us

profile of v2, /device:TPU:0, one launch (start us, length us, event | category | flops | bytes accessed | tf_op | source)
XLA Modules:
  0.0 145.0 jit_solution(3739842584683423318)
XLA Ops:
  0.6 0.0 copy-start
  0.6 0.0 copy-start.9
  0.7 0.8 convert_convert_fusion
  1.5 0.8 slice_bitcast_fusion.5
  2.3 0.1 select_reduce_fusion.4
  2.4 0.8 convert_add_fusion
  3.2 0.2 select_reduce_fusion.2
  3.4 0.1 convert_element_type.187
  3.5 1.1 copy.24
  4.6 0.2 copy.25
  4.8 0.0 copy-start.1
  4.8 1.3 convolution_convert_fusion.3
  6.2 0.0 copy-done.9
  6.2 0.3 convolution_convert_fusion.4
  6.5 0.1 fusion.10
  6.6 0.0 copy-done.1
  6.6 65.8 %dispatch.1 = (bf16[4,8,40,2176]{3,2,1,0:T(8,128)(2,1)S(1)}, bf16[8,128,1024]{2,1,0:T(8,128)(2,1)S(1)}, bf16[8,128,128]{2,1,0:T(8,128)(2,1)S(1)}) custom-call(bf16[8,40,2176]{2,1,0:T(8,128)(2,1)S(1)} %bitcast.100, bf16[128,1024]{1,0:T(8,128)(2,1)S(1)} %copy-done.1, bf16[8,128,128]{2,1,0:T(8,128)(2,1)S(1)} %bitcast.103), custom_call_target="tpu_custom_call" | custom-call | tf_op jit(solution)/shard_map/dispatch/pallas_call | solution.py:171
  72.5 1.3 convolution_bitcast_fusion
  73.7 0.1 convert_reduce_fusion
  73.9 3.1 %slice_bitcast_fusion = (bf16[1,8,40,4,1024]{4,2,1,3,0:T(8,128)(2,1)}, bf16[1,8,40,4,1024]{4,2,1,3,0:T(8,128)(2,1)}) fusion(bf16[4,8,40,2176]{3,2,1,0:T(8,128)(2,1)S(1)} %get-tuple-element.9), kind=kLoop, calls=%fused_computation.9 | loop fusion | bytes 10485760 | tf_op jit(solution)/shard_map/transpose | solution.py:318
  76.9 0.1 reshape.261
  77.0 3.8 %copy.27 = bf16[1,8,40,4,1024]{4,3,2,1,0:T(4,128)(2,1)S(1)} copy(bf16[1,8,40,4,1024]{4,2,1,3,0:T(8,128)(2,1)} %get-tuple-element.18) | data formatting | bytes 5242880 | tf_op jit(solution)/shard_map/transpose | solution.py:318
  80.8 0.0 copy-start.5
  80.8 1.1 copy.35
  81.9 0.0 copy-start.2
  81.9 0.4 copy-done.5
  82.4 0.0 copy-start.7
  82.4 0.9 fusion.4
  83.2 0.2 copy-done.2
  83.5 1.0 copy-done.7
  84.4 0.0 copy-start.4
  84.4 0.9 fusion.6
  85.3 0.9 copy-done.4
  86.2 2.0 %copy.26 = bf16[1,8,40,4,1024]{4,3,2,1,0:T(4,128)(2,1)S(1)} copy(bf16[1,8,40,4,1024]{4,2,1,3,0:T(8,128)(2,1)S(1)} %copy-done.4) | data formatting | bytes 5242880 | tf_op jit(solution)/shard_map/transpose | solution.py:318
  88.2 1.1 copy.34
  89.4 0.0 copy-done
  89.4 1.4 fusion.36
  90.8 2.7 %fusion.2 = bf16[1,256,4096]{2,1,0:T(8,128)(2,1)} fusion(bf16[320,4096]{1,0:T(8,128)(2,1)S(1)} %bitcast.109, bf16[320,256]{1,0:T(8,128)(2,1)S(1)} %get-tuple-element.17, f32[320]{0:T(512)S(1)} %reshape.261), kind=kOutput, calls=%fused_computation.5 | convolution fusion | flops 672382976 | bytes 4883712 | tf_op jit(solution)/shard_map/lrf,lrd->lfd/dot_general | solution.py:358
  93.5 0.2 copy.33
  93.6 0.0 copy-start.8
  93.7 0.0 copy-start.6
  93.7 1.5 %fusion.17 = f32[320,1024]{1,0:T(8,128)S(1)} fusion(bf16[320,256]{1,0:T(8,128)(2,1)S(1)} %get-tuple-element.20, bf16[1,256,4096]{2,1,0:T(8,128)(2,1)} %param.12), kind=kOutput, calls=%fused_computation.32 | convolution fusion | flops 167772160 | bytes 1998848 | tf_op jit(solution)/shard_map/lrf,lfd->lrd/dot_general | solution.py:342
  95.2 0.2 copy-done.8
  95.4 0.3 fusion.14
  95.7 0.3 copy-done.6
  96.0 0.3 fusion.20
  96.4 0.3 fusion.13
  96.7 0.3 fusion.23
  97.1 0.3 fusion.12
  97.4 0.3 fusion.26
  97.8 0.3 fusion.11
  98.1 0.3 maximum_maximum_fusion.blocks
  98.4 37.5 %combine.1 = bf16[8,40,1280]{2,1,0:T(8,128)(2,1)S(1)} custom-call(bf16[4,8,40,1152]{3,2,1,0:T(8,128)(2,1)S(1)} %maximum_maximum_fusion.blocks), custom_call_target="tpu_custom_call" | custom-call | tf_op jit(solution)/shard_map/combine/pallas_call | solution.py:244
  136.0 1.0 convolution_convert_fusion.5
  137.0 0.2 copy.32
  137.2 0.1 select_reduce_fusion.1
  137.3 0.6 pad_maximum_fusion.1
  137.9 0.0 copy-start.3
  137.9 4.5 %fusion.1 = bf16[1,256,4096]{2,1,0:T(8,128)(2,1)} fusion(bf16[320,256]{1,0:T(8,128)(2,1)S(1)} %get-tuple-element.21, bf16[320,4096]{1,0:T(8,128)(2,1)} %bitcast.106), kind=kOutput, calls=%fused_computation.4 | convolution fusion | flops 672137216 | bytes 4882432 | tf_op jit(solution)/shard_map/lrf,lrd->lfd/dot_general | solution.py:355
  142.4 0.0 copy-done.3
  142.4 2.6 %fusion = bf16[1,256,4096]{2,1,0:T(8,128)(2,1)} fusion(bf16[320,256]{1,0:T(8,128)(2,1)S(1)} %get-tuple-element.20, bf16[320,4096]{1,0:T(8,128)(2,1)S(1)} %bitcast.107), kind=kOutput, calls=%fused_computation.3 | convolution fusion | flops 672137216 | bytes 4882432 | tf_op jit(solution)/shard_map/lrf,lrd->lfd/dot_general | solution.py:352
  (8 shorter events, 0.1 us)
Async XLA Ops:
  0.6 88.7 %copy-start = (bf16[1,256,4096]{2,1,0:T(8,128)(2,1)S(1)}, bf16[1,256,4096]{2,1,0:T(8,128)(2,1)}, u32[]{:S(2)}) copy-start(bf16[1,256,4096]{2,1,0:T(8,128)(2,1)} %param.14) | copy-start | bytes 6291460
  0.6 5.5 %copy-start.9 = (bf16[128,1024]{1,0:T(8,128)(2,1)S(1)}, bf16[128,1024]{1,0:T(8,128)(2,1)}, u32[]{:S(2)}) copy-start(bf16[128,1024]{1,0:T(8,128)(2,1)} %param.8) | copy-start | bytes 786436
  4.8 1.8 %copy-start.1 = (bf16[128,1024]{1,0:T(8,128)(2,1)S(1)}, bf16[128,1024]{1,0:T(8,128)(2,1)}, u32[]{:S(2)}) copy-start(bf16[128,1024]{1,0:T(8,128)(2,1)} %grads.1) | copy-start | bytes 786436
  80.8 1.6 %copy-start.5 = (bf16[1,256,4096]{2,1,0:T(8,128)(2,1)S(1)}, bf16[1,256,4096]{2,1,0:T(8,128)(2,1)}, u32[]{:S(2)}) copy-start(bf16[1,256,4096]{2,1,0:T(8,128)(2,1)} %param.12) | copy-start | bytes 6291460
  81.9 1.5 %copy-start.2 = (bf16[40,8,4,1024]{3,1,2,0:T(8,128)(2,1)}, bf16[40,8,4,1024]{3,1,2,0:T(8,128)(2,1)S(1)}, u32[]{:S(2)}) copy-start(bf16[40,8,4,1024]{3,1,2,0:T(8,128)(2,1)S(1)} %copy.35) | copy-start | bytes 7864324
  82.4 2.1 %copy-start.7 = (bf16[1,256,4096]{2,1,0:T(8,128)(2,1)S(1)}, bf16[1,256,4096]{2,1,0:T(8,128)(2,1)}, u32[]{:S(2)}) copy-start(bf16[1,256,4096]{2,1,0:T(8,128)(2,1)} %param.13) | copy-start | bytes 6291460
  84.4 1.7 %copy-start.4 = (bf16[1,8,40,4,1024]{4,2,1,3,0:T(8,128)(2,1)S(1)}, bf16[1,8,40,4,1024]{4,2,1,3,0:T(8,128)(2,1)}, u32[]{:S(2)}) copy-start(bf16[1,8,40,4,1024]{4,2,1,3,0:T(8,128)(2,1)} %get-tuple-element.19) | copy-start | bytes 7864324
  93.6 1.8 %copy-start.8 = (bf16[1,256,4096]{2,1,0:T(8,128)(2,1)S(1)}, bf16[1,256,4096]{2,1,0:T(8,128)(2,1)}, u32[]{:S(2)}) copy-start(bf16[1,256,4096]{2,1,0:T(8,128)(2,1)} %param.13) | copy-start | bytes 6291460
  93.7 2.4 %copy-start.6 = (bf16[1,256,4096]{2,1,0:T(8,128)(2,1)S(1)}, bf16[1,256,4096]{2,1,0:T(8,128)(2,1)}, u32[]{:S(2)}) copy-start(bf16[1,256,4096]{2,1,0:T(8,128)(2,1)} %param.12) | copy-start | bytes 6291460
  137.9 4.5 %copy-start.3 = (bf16[40,8,4,1024]{3,1,2,0:T(8,128)(2,1)S(1)}, bf16[40,8,4,1024]{3,1,2,0:T(8,128)(2,1)}, u32[]{:S(2)}) copy-start(bf16[40,8,4,1024]{3,1,2,0:T(8,128)(2,1)} %copy-done.2) | copy-start | bytes 7864324
